TPU v7x, 256 devices: a whole 4x4x8 slice. The times are simulated.
256 devices in a mesh: kv: 16 (over y, x), tp: 16 (over z, core).
Axes of the slice: x: 4, y: 4, z: 8, core: 2. Of those that a mesh axis runs over, the one named last changes fastest.
Arguments:
- tokens: bfloat16 [1536, 4096], P('kv', 'tp'), may hold values from -20 to 20
- state: float32 [1536, 32, 4096], P('kv', 'tp'), may hold values from -4 to 4
- w_query: bfloat16 [4096, 2048], P(None, 'tp'), may hold values from -0.09375 to 0.09375
- w_key: bfloat16 [4096, 2048], P(None, 'tp'), may hold values from -0.09375 to 0.09375
- w_value: bfloat16 [4096, 2048], P(None, 'tp'), may hold values from -0.09375 to 0.09375
- w_gate: bfloat16 [4096, 2048], P(None, 'tp'), may hold values from -0.09375 to 0.09375
- w_decay: bfloat16 [4096, 32], replicated, may hold values from -0.09375 to 0.09375
- w_beta: bfloat16 [4096, 32], replicated, may hold values from -0.09375 to 0.09375
- decay_rate: float32 [32], P('tp'), may hold values from 0.03 to 3
- decay_bias: float32 [32], P('tp'), may hold values from -1 to 1
- mix_gain: float32 [4096], replicated, may hold values from 0.1 to 1.9
- out_gain: float32 [64], replicated, may hold values from 0.1 to 1.9
- w_out: bfloat16 [2048, 4096], P('tp'), may hold values from -0.125 to 0.125
- ffn_gain: float32 [4096], replicated, may hold values from 0.1 to 1.9
- w_up: bfloat16 [4096, 16384], P('tp', 'kv'), may hold values from -0.09375 to 0.09375
- w_down: bfloat16 [16384, 4096], P('kv', 'tp'), may hold values from -0.046875 to 0.046875
Outputs:
- mixed: bfloat16 [1536, 4096], P('kv', 'tp')
- new_state: float32 [1536, 32, 4096], P('kv', 'tp')
All inputs are finite; a program needn't handle non-finite values.
Results may differ from a plain program's by a relative error of at most 0.024.
Values may be sent and summed in bfloat16 or wider, within the bound.
No kernel may reach another device: no remote copies, remote signals or barrier semaphores. Data moves between devices by JAX's collectives and lax.ppermute only.
A program may use at most 64 MiB of HBM per device.

v0:
```python
import jax
import jax.numpy as jnp
from jax import lax
from jax.sharding import Mesh
from jax.sharding import PartitionSpec as P

D = 4096
HEAD_DIM = 64
TP = ("tp_0", "tp_1")
EPS = 1e-06


def sent_to_all(array, axis):
    length = lax.axis_size(axis)
    return lax.all_to_all(
        jnp.broadcast_to(array[None], (length, *array.shape)), axis, 0, 0, tiled=True
    )


def joined_along(parts, dim):
    dims = list(parts.shape[1:])
    dims[dim] *= parts.shape[0]
    return jnp.moveaxis(parts, 0, dim).reshape(dims)


def gathered_copies(array, axis, dim):
    parts = sent_to_all(array, axis)
    return joined_along(parts, dim)


def in_blocks(array, dim, length):
    before, after = (array.shape[:dim], array.shape[dim + 1 :])
    return jnp.moveaxis(array.reshape(*before, length, -1, *after), dim, 0)


def sum_at_owner(array, axis, dim):
    parts = in_blocks(array, dim, lax.axis_size(axis))
    arrived = lax.all_to_all(parts, axis, split_axis=0, concat_axis=0, tiled=True)
    return arrived.astype(jnp.float32).sum(axis=0)


def over_copies(array, axis):
    everything = sent_to_all(array, axis)
    return jnp.sum(everything, axis=0)


def scatter_pairs(array, chips, core, dim):
    sizes = (lax.axis_size(chips), lax.axis_size(core))
    parts = in_blocks(array, dim, sizes[0] * sizes[1])
    inside = parts.shape[1:]
    parts = parts.reshape(*sizes, *inside).swapaxes(0, 1).reshape(-1, *inside)
    parts = lax.psum_scatter(parts, core, scatter_dimension=0, tiled=True)
    return lax.psum_scatter(parts, chips, scatter_dimension=0, tiled=True)[0]


def unit_norm(vector):
    return vector * lax.rsqrt(jnp.sum(vector * vector, axis=-1, keepdims=True) + EPS)


def local(
    tokens,
    state,
    w_query,
    w_key,
    w_value,
    w_gate,
    w_decay,
    w_beta,
    decay_rate,
    decay_bias,
    mix_gain,
    out_gain,
    w_out,
    ffn_gain,
    w_up,
    w_down,
):
    rows = tokens.shape[0]
    width_share = tokens.shape[1]
    head_count = w_query.shape[1] // HEAD_DIM
    full_rows = gathered_copies(tokens, TP, 1)
    full_f = full_rows.astype(jnp.float32)
    normed = (
        full_f * lax.rsqrt(jnp.mean(full_f * full_f, axis=-1, keepdims=True) + EPS) * mix_gain
    ).astype(jnp.bfloat16)
    query = jnp.dot(normed, w_query, preferred_element_type=jnp.float32).reshape(
        rows, head_count, HEAD_DIM
    )
    key_proj = jnp.dot(normed, w_key, preferred_element_type=jnp.float32).reshape(
        rows, head_count, HEAD_DIM
    )
    value = jnp.dot(normed, w_value, preferred_element_type=jnp.float32).reshape(
        rows, head_count, HEAD_DIM
    )
    gate = jnp.dot(normed, w_gate, preferred_element_type=jnp.float32).reshape(
        rows, head_count, HEAD_DIM
    )
    query = unit_norm(query) * HEAD_DIM ** (-0.5)
    key_proj = unit_norm(key_proj)
    head_start = lax.axis_index(TP) * head_count
    decay_cols = lax.dynamic_slice_in_dim(w_decay, head_start, head_count, 1)
    beta_cols = lax.dynamic_slice_in_dim(w_beta, head_start, head_count, 1)
    pre_decay = jnp.dot(normed, decay_cols, preferred_element_type=jnp.float32)
    decay = jnp.exp(-decay_rate * jax.nn.softplus(pre_decay + decay_bias))
    strength = jax.nn.sigmoid(jnp.dot(normed, beta_cols, preferred_element_type=jnp.float32))
    matrix = state.reshape(rows, head_count, HEAD_DIM, HEAD_DIM) * decay[:, :, None, None]
    recalled = jnp.einsum("bhk,bhkv->bhv", key_proj, matrix, precision=lax.Precision.HIGHEST)
    delta = (value - recalled) * strength[:, :, None]
    matrix = matrix + key_proj[:, :, :, None] * delta[:, :, None, :]
    head_out = jnp.einsum("bhk,bhkv->bhv", query, matrix, precision=lax.Precision.HIGHEST)
    head_out = (
        head_out
        * lax.rsqrt(jnp.mean(head_out * head_out, axis=-1, keepdims=True) + EPS)
        * out_gain
        * jax.nn.silu(gate)
    )
    head_out = head_out.reshape(rows, head_count * HEAD_DIM).astype(jnp.bfloat16)
    partial_value = jnp.dot(head_out, w_out, preferred_element_type=jnp.float32)
    feature_start = lax.axis_index(TP) * width_share
    gain_share = lax.dynamic_slice_in_dim(ffn_gain, feature_start, width_share, 0)
    resid = tokens.astype(jnp.float32) + sum_at_owner(partial_value.astype(jnp.bfloat16), TP, 1)
    squares = over_copies(jnp.sum(resid * resid, axis=-1), TP)
    scale = lax.rsqrt(squares[:, None] / D + EPS)
    ffn_in = (resid * scale * gain_share).astype(jnp.bfloat16)
    up_part = jnp.dot(gathered_copies(ffn_in, "kv", 0), w_up, preferred_element_type=jnp.float32)
    up_share = scatter_pairs(up_part.astype(jnp.bfloat16), "tp_0", "tp_1", 0).astype(jnp.float32)
    hidden_share = jnp.square(jax.nn.relu(up_share)).astype(jnp.bfloat16)
    hidden = lax.all_gather(hidden_share, TP, axis=0, tiled=True)
    down = sum_at_owner(
        jnp.dot(hidden, w_down, preferred_element_type=jnp.float32).astype(jnp.bfloat16), "kv", 0
    )
    mixed = (resid + down).astype(jnp.bfloat16)
    return (mixed, matrix.reshape(rows, head_count, HEAD_DIM * HEAD_DIM))


def solution(mesh):
    split = Mesh(mesh.devices.reshape(mesh.shape["kv"], 8, 2), ("kv", "tp_0", "tp_1"))
    placed = (
        P("kv", TP),
        P("kv", TP, None),
        P(None, TP),
        P(None, TP),
        P(None, TP),
        P(None, TP),
        P(),
        P(),
        P(TP),
        P(TP),
        P(),
        P(),
        P(TP, None),
        P(),
        P(TP, "kv"),
        P("kv", TP),
    )
    return jax.shard_map(
        local,
        mesh=split,
        in_specs=placed,
        out_specs=(P("kv", TP), P("kv", TP, None)),
        check_vma=False,
    )
```

profile of v0, /device:TPU:1, one launch (start us, length us, event | category | flops | bytes accessed | tf_op | source)
XLA Modules:
  0.0 243.3 jit_solution(4121412433545076519)
XLA Ops:
  7.2 0.0 copy-start
  7.2 1.9 broadcast_in_dim.6
  9.1 10.0 %all-to-all-start = ((bf16[16,96,256]{2,1,0:T(8,128)(2,1)}), bf16[16,96,256]{2,1,0:T(8,128)(2,1)S(1)}, u32[]{:S(2)}, u32[]{:S(2)}) async-start(bf16[16,96,256]{2,1,0:T(8,128)(2,1)} %broadcast_in_dim.6), calls=%async_computation | async-start | bytes 1572864 | tf_op jit(solution)/shard_map/all_to_all | solution.py:15
  19.1 0.7 mul.175
  19.8 1.3 copy.69
  21.1 2.3 copy.66
  23.4 0.0 copy-done.12
  23.4 6.1 %copy.67 = f32[96,2,4096]{0,2,1:T(8,128)} copy(f32[96,2,4096]{2,1,0:T(2,128)} %param.17) | data formatting | bytes 6291456 | tf_op args[1]
  29.5 1.3 copy.70
  30.8 2.3 copy.71
  33.1 8.7 %all-to-all-done = bf16[16,96,256]{2,1,0:T(8,128)(2,1)S(1)} async-done(((bf16[16,96,256]{2,1,0:T(8,128)(2,1)}), bf16[16,96,256]{2,1,0:T(8,128)(2,1)S(1)}, u32[]{:S(2)}, u32[]{:S(2)}) %all-to-all-start) | async-done | bytes 786464 | tf_op jit(solution)/shard_map/all_to_all | solution.py:15
  41.8 0.3 fusion.5
  42.0 0.3 fusion.12
  42.3 0.4 copy.65
  42.8 0.4 reshape.142
  43.1 1.7 multiply_reduce_fusion.4
  44.8 1.7 multiply_reduce_fusion.5
  46.5 0.0 copy-start.8
  46.5 0.0 copy-start.9
  46.5 0.2 convert_bitcast_fusion
  46.7 0.2 copy.90
  46.9 0.4 copy-done.8
  47.2 1.5 fusion.11
  48.7 0.0 copy-start.2
  48.7 1.3 fusion.16
  50.1 0.6 multiply_reduce_fusion.1
  50.7 0.5 fusion.8
  51.2 0.0 copy-start.3
  51.2 0.0 copy-start.10
  51.2 3.0 %broadcast_multiply_fusion = (f32[96,2,64,64]{0,3,2,1:T(8,128)}, f32[96,2,64]{0,2,1:T(8,128)S(1)}) fusion(f32[96,2,64]{0,2,1:T(8,128)S(1)} %fusion.8, f32[96,2,64]{0,2,1:T(8,128)S(1)} %get-tuple-element.19, f32[96,2,64,64]{0,3,2,1:T(8,128)S(1)} %bitcast.55, f32[96,2]{0,1:T(2,128)S(1)} %fusion.16, f32[96,2,64]{0,2,1:T(8,128)S(1)} %get-tuple-element.18), kind=kLoop, calls=%fused_computation.11 | loop fusion | flops 3919872 | bytes 6488832 | tf_op jit(solution)/shard_map/mul | solution.py:109
  54.3 0.4 multiply_convert_fusion.3
  54.8 0.0 copy-start.6
  54.8 0.4 convolution_convert_fusion
  55.2 0.0 copy-start.7
  55.2 0.1 copy.92
  55.3 25.8 %all_to_all.26 = bf16[16,96,256]{2,1,0:T(8,128)(2,1)S(1)} all-to-all(bf16[16,96,256]{2,1,0:T(8,128)(2,1)S(1)} %bitcast.66), channel_id=1, replica_groups=mesh['kv'=16,'tp_0'=8,'tp_1'=2] {'tp_0','tp_1'}, dimensions={0} | all-to-all | bytes 1572864 | tf_op jit(solution)/shard_map/all_to_all | solution.py:38
  81.1 0.1 convert_reduce_fusion.1
  81.2 0.1 multiply_reduce_fusion.2
  81.3 0.6 broadcast_in_dim.7
  82.0 3.4 %all-to-all-start.2 = ((f32[16,1,96]{2,1,0:T(1,128)}), f32[16,1,96]{2,1,0:T(1,128)S(1)}, u32[]{:S(2)}, u32[]{:S(2)}) async-start(f32[16,1,96]{2,1,0:T(1,128)} %broadcast_in_dim.7), calls=%async_computation.2 | async-start | bytes 16384 | tf_op jit(solution)/shard_map/all_to_all | solution.py:15
  85.3 0.0 reduce-scatter.3.cloned.1.call-start
  85.4 0.8 dynamic_slice.11
  86.2 5.8 %all-to-all-done.2 = f32[16,1,96]{2,1,0:T(1,128)S(1)} async-done(((f32[16,1,96]{2,1,0:T(1,128)}), f32[16,1,96]{2,1,0:T(1,128)S(1)}, u32[]{:S(2)}, u32[]{:S(2)}) %all-to-all-start.2) | async-done | bytes 6176 | tf_op jit(solution)/shard_map/all_to_all | solution.py:15
  91.9 0.1 multiply_convert_fusion.2
  92.0 0.1 broadcast_in_dim.8
  92.1 20.1 %all_to_all.27 = bf16[16,96,256]{2,1,0:T(8,128)(2,1)S(1)} all-to-all(bf16[16,96,256]{2,1,0:T(8,128)(2,1)S(1)} %broadcast_in_dim.8), channel_id=1, replica_groups=mesh['kv'=16,'tp_0'=8,'tp_1'=2] {'kv'}, dimensions={0} | all-to-all | bytes 1572864 | tf_op jit(solution)/shard_map/all_to_all | solution.py:15
  112.2 1.0 convolution_convert_fusion.1
  113.2 2.1 copy.74
  115.3 0.0 reduce-scatter.3.cloned.1.call-update
  115.3 0.0 reduce-scatter.5.cloned.1.call-start
  115.4 10.4 %reduce-scatter.3.cloned.1.call-done = bf16[8,96,1024]{2,1,0:T(8,128)(2,1)} async-done(((bf16[16,96,1024]{2,1,0:T(8,128)(2,1)}), bf16[8,96,1024]{2,1,0:T(8,128)(2,1)}) %reduce-scatter.3.cloned.1.call-update) | async-done | bytes 1572880 | tf_op jit(solution)/shard_map/reduce_scatter | solution.py:52
  125.7 0.0 reduce-scatter.5.cloned.1.call-update
  125.8 0.0 all-gather.3.cloned.1.call-start
  125.8 40.4 %reduce-scatter.5.cloned.1.call-done = bf16[1,96,1024]{2,1,0:T(8,128)(2,1)} async-done(((bf16[8,96,1024]{2,1,0:T(8,128)(2,1)}), bf16[1,96,1024]{2,1,0:T(8,128)(2,1)}) %reduce-scatter.5.cloned.1.call-update) | async-done | bytes 196624 | tf_op jit(solution)/shard_map/reduce_scatter | solution.py:53
  166.2 1.6 multiply_convert_fusion.1
  167.9 0.0 all-gather.3.cloned.1.call-update
  167.9 44.2 %all-gather.3.cloned.1.call-done = bf16[1,1536,1024]{2,1,0:T(8,128)(2,1)} async-done(((bf16[1,96,1024]{2,1,0:T(8,128)(2,1)}), bf16[1,1536,1024]{2,1,0:T(8,128)(2,1)}) %all-gather.3.cloned.1.call-update) | async-done | bytes 3145744 | tf_op jit(solution)/shard_map/all_gather | solution.py:128
  212.1 3.8 %fusion.2 = bf16[1536,256]{1,0:T(8,128)(2,1)} fusion(bf16[1024,256]{1,0:T(8,128)(2,1)S(1)} %copy-done.11, bf16[1,1536,1024]{2,1,0:T(8,128)(2,1)} %all-gather.3.cloned.1.call-done), kind=kOutput, calls=%fused_computation.7 | convolution fusion | flops 805699584 | bytes 4456448 | tf_op jit(solution)/shard_map/dot_general | solution.py:130
  215.9 6.5 %all-to-all-start.4 = ((bf16[16,96,256]{2,1,0:T(8,128)(2,1)}), bf16[16,96,256]{2,1,0:T(8,128)(2,1)S(1)}, u32[]{:S(2)}, u32[]{:S(2)}) async-start(bf16[16,96,256]{2,1,0:T(8,128)(2,1)} %bitcast.19), calls=%async_computation.6 | async-start | bytes 1572864 | tf_op jit(solution)/shard_map/all_to_all | solution.py:38
  222.4 5.8 %bitcast_add_fusion = f32[96,2,4096]{0,2,1:T(8,128)} fusion(f32[96,2,64,64]{0,3,2,1:T(8,128)} %get-tuple-element.12, f32[96,2,4096]{0,2,1:T(8,128)} %copy.67, f32[96,2]{0,1:T(2,128)S(1)} %fusion.16), kind=kLoop, calls=%fused_computation.1 | loop fusion | flops 1572864 | bytes 9437952 | tf_op jit(solution)/shard_map/add | solution.py:109
  228.2 6.0 %copy.76 = f32[96,2,4096]{2,1,0:T(2,128)} copy(f32[96,2,4096]{0,2,1:T(8,128)} %bitcast_add_fusion) | data formatting | bytes 6291456
  234.2 1.8 all-to-all-done.4
  236.0 0.1 convert_reduce_fusion
  236.2 0.6 add_convert_fusion
  (25 shorter events, 0.1 us)
Async XLA Ops:
  7.2 47.6 %copy-start = (bf16[128,4096]{1,0:T(8,128)(2,1)S(1)}, bf16[128,4096]{1,0:T(8,128)(2,1)}, u32[]{:S(2)}) copy-start(bf16[128,4096]{1,0:T(8,128)(2,1)} %param.28) | copy-start | bytes 3145732
  7.2 12.6 %copy-start.4 = (bf16[4096,128]{1,0:T(8,128)(2,1)S(1)}, bf16[4096,128]{1,0:T(8,128)(2,1)}, u32[]{:S(2)}) copy-start(bf16[4096,128]{1,0:T(8,128)(2,1)} %param.19) | copy-start | bytes 3145732
  7.2 16.2 %copy-start.12 = (f32[2]{0:T(128)S(1)}, f32[2]{0:T(128)}, u32[]{:S(2)}) copy-start(f32[2]{0:T(128)} %param.24) | copy-start | bytes 28
  9.1 32.7 %all-to-all-start = ((bf16[16,96,256]{2,1,0:T(8,128)(2,1)}), bf16[16,96,256]{2,1,0:T(8,128)(2,1)S(1)}, u32[]{:S(2)}, u32[]{:S(2)}) async-start(bf16[16,96,256]{2,1,0:T(8,128)(2,1)} %broadcast_in_dim.6), calls=%async_computation | async-start | bytes 1572864 | tf_op jit(solution)/shard_map/all_to_all | solution.py:15
  23.4 6.1 %copy-start.5 = (bf16[4096,128]{1,0:T(8,128)(2,1)S(1)}, bf16[4096,128]{1,0:T(8,128)(2,1)}, u32[]{:S(2)}) copy-start(bf16[4096,128]{1,0:T(8,128)(2,1)} %param.20) | copy-start | bytes 3145732
  46.5 0.7 copy-start.8
  46.5 2.2 copy-start.9
  46.7 3.4 %copy-start.1 = (f32[96,2,4096]{0,2,1:T(8,128)S(1)}, f32[96,2,4096]{0,2,1:T(8,128)}, u32[]{:S(2)}) copy-start(f32[96,2,4096]{0,2,1:T(8,128)} %copy.67) | copy-start | bytes 9437188
  48.7 2.0 copy-start.2
  51.2 3.1 %copy-start.3 = (bf16[4096,128]{0,1:T(8,128)(2,1)S(1)}, bf16[4096,128]{0,1:T(8,128)(2,1)}, u32[]{:S(2)}) copy-start(bf16[4096,128]{0,1:T(8,128)(2,1)} %copy.71) | copy-start | bytes 3145732
  51.2 3.1 %copy-start.10 = (f32[64]{0:T(128)S(1)}, f32[64]{0:T(128)}, u32[]{:S(2)}) copy-start(f32[64]{0:T(128)} %param.27) | copy-start | bytes 772
  54.8 26.5 %copy-start.6 = (bf16[96,256]{1,0:T(8,128)(2,1)S(1)}, bf16[96,256]{1,0:T(8,128)(2,1)}, u32[]{:S(2)}) copy-start(bf16[96,256]{1,0:T(8,128)(2,1)} %param.16) | copy-start | bytes 147460
  55.2 57.0 %copy-start.7 = (bf16[256,1024]{1,0:T(8,128)(2,1)S(1)}, bf16[256,1024]{1,0:T(8,128)(2,1)}, u32[]{:S(2)}) copy-start(bf16[256,1024]{1,0:T(8,128)(2,1)} %param.30) | copy-start | bytes 1572868
  82.0 10.0 %all-to-all-start.2 = ((f32[16,1,96]{2,1,0:T(1,128)}), f32[16,1,96]{2,1,0:T(1,128)S(1)}, u32[]{:S(2)}, u32[]{:S(2)}) async-start(f32[16,1,96]{2,1,0:T(1,128)} %broadcast_in_dim.7), calls=%async_computation.2 | async-start | bytes 16384 | tf_op jit(solution)/shard_map/all_to_all | solution.py:15
  85.3 40.4 %reduce-scatter.3.cloned.1.call-start = ((), (), s32[]{:S(2)}) async-start(), calls=%async_computation.7 | async-start | bytes 4718592 | tf_op jit(solution)/shard_map/reduce_scatter | solution.py:52
  115.3 96.8 %copy-start.11 = (bf16[1024,256]{1,0:T(8,128)(2,1)S(1)}, bf16[1024,256]{1,0:T(8,128)(2,1)}, u32[]{:S(2)}) copy-start(bf16[1024,256]{1,0:T(8,128)(2,1)} %param.31) | copy-start | bytes 1572868
  115.3 50.9 %reduce-scatter.5.cloned.1.call-start = ((), (), s32[]{:S(2)}) async-start(), calls=%async_computation.8 | async-start | bytes 1769472 | tf_op jit(solution)/shard_map/reduce_scatter | solution.py:53
  125.8 86.4 %all-gather.3.cloned.1.call-start = ((), (), s32[]{:S(2)}) async-start(), calls=%async_computation.9 | async-start | bytes 3342336 | tf_op jit(solution)/shard_map/all_gather | solution.py:128
  215.9 20.2 %all-to-all-start.4 = ((bf16[16,96,256]{2,1,0:T(8,128)(2,1)}), bf16[16,96,256]{2,1,0:T(8,128)(2,1)S(1)}, u32[]{:S(2)}, u32[]{:S(2)}) async-start(bf16[16,96,256]{2,1,0:T(8,128)(2,1)} %bitcast.19), calls=%async_computation.6 | async-start | bytes 1572864 | tf_op jit(solution)/shard_map/all_to_all | solution.py:38
Sparse Core Ops, SparseCore 0:
  115.5 10.2 reduce-scatter.2
  128.3 37.8 reduce-scatter.4
  168.6 43.4 all-gather.2
where the time goes:
time: 244 us; the launch traced here: 243 us
  waiting for transfers between devices  111 us (45%)
  blocking collectives  45.9 us (19%)
  local copies, waits for them, and re-layouts  26.8 us (11%)
  starting transfers between devices  20 us (8%)
  between operations  14 us (6%)
  other arithmetic  12.9 us (5%)
  matrix products  12.2 us (5%)
    all_gather x1, waiting for transfers between devices, local(): hidden = lax.all_gather(hidden_share, TP, axis=0, tiled=True)  44.2 us
    reduce_scatter x1, waiting for transfers between devices, scatter_pairs(): return lax.psum_scatter(parts, chips, scatter_dimension=0, tiled=True)[0]  40.4 us
    all_to_all x1, blocking collectives, sum_at_owner(): lax.all_to_all(parts, axis, split_axis=0, concat_axis=0, tiled=True)  25.8 us
    all_to_all x1, blocking collectives, sent_to_all(): lax.all_to_all(jnp.broadcast_to(array[None], (length, *array.shape)), axi...  20.1 us
    unnamed x32, local copies, waits for them, and re-layouts  19.7 us
    all_to_all x2, waiting for transfers between devices, sent_to_all(): lax.all_to_all(jnp.broadcast_to(array[None], (length, *array.shape)), axi...  14.5 us
    all_to_all x2, starting transfers between devices, sent_to_all(): lax.all_to_all(jnp.broadcast_to(array[None], (length, *array.shape)), axi...  13.3 us
    reduce_scatter x1, waiting for transfers between devices, scatter_pairs(): parts = lax.psum_scatter(parts, core, scatter_dimension=0, tiled=True)  10.4 us
  transfers between devices with their start and end apart: 6, of which 6 were waited for; matrix products, arithmetic and copies ran while one was open for 11% of the time, Pallas kernels for 0%

commit v1 on v0

--- a/solution.py
+++ b/solution.py
@@ -125,7 +125,8 @@
     up_part = jnp.dot(gathered_copies(ffn_in, "kv", 0), w_up, preferred_element_type=jnp.float32)
     up_share = scatter_pairs(up_part.astype(jnp.bfloat16), "tp_0", "tp_1", 0).astype(jnp.float32)
     hidden_share = jnp.square(jax.nn.relu(up_share)).astype(jnp.bfloat16)
-    hidden = lax.all_gather(hidden_share, TP, axis=0, tiled=True)
+    sent = jnp.stack([hidden_share] * lax.axis_size(TP))
+    hidden = jnp.concatenate(lax.all_to_all(sent, TP, 0, 0), axis=0)
     down = sum_at_owner(
         jnp.dot(hidden, w_down, preferred_element_type=jnp.float32).astype(jnp.bfloat16), "kv", 0
     )

time: 244 us -> 281 us (1.15)
  blocking collectives: 45.9 us -> 128 us
  waiting for transfers between devices: 111 us -> 68.1 us
    all_to_all x0 -> x1, blocking collectives: none -> 82.3 us  [local(): hidden = jnp.concatenate(lax.all_to_all(sent, TP, 0, 0), axis=0)]
    all_gather x1 -> x0, waiting for transfers between devices: 44.2 us -> none  [local(): hidden = lax.all_gather(hidden_share, TP, axis=0, tiled=True)]
  transfers between devices with their start and end apart: 6 -> 5, of which waited for: 6 -> 5; matrix products, arithmetic and copies ran while one was open for 11% -> 9% of each run, Pallas kernels for 0% -> 0%
where the time goes in v1:
time: 281 us
  blocking collectives  128 us (46%)
  waiting for transfers between devices  68.1 us (24%)
  local copies, waits for them, and re-layouts  27.2 us (10%)
  starting transfers between devices  19.9 us (7%)
  between operations  14.4 us (5%)
  other arithmetic  12.2 us (4%)
  matrix products  10.4 us (4%)
    all_to_all x1, blocking collectives, local(): hidden = jnp.concatenate(lax.all_to_all(sent, TP, 0, 0), axis=0)  82.3 us
    reduce_scatter x1, waiting for transfers between devices, scatter_pairs(): return lax.psum_scatter(parts, chips, scatter_dimension=0, tiled=True)[0]  40.5 us
    all_to_all x1, blocking collectives, sum_at_owner(): lax.all_to_all(parts, axis, split_axis=0, concat_axis=0, tiled=True)  25.8 us
    all_to_all x1, blocking collectives, sent_to_all(): lax.all_to_all(jnp.broadcast_to(array[None], (length, *array.shape)), axi...  20.1 us
    unnamed x32, local copies, waits for them, and re-layouts  19.7 us
    all_to_all x2, waiting for transfers between devices, sent_to_all(): lax.all_to_all(jnp.broadcast_to(array[None], (length, *array.shape)), axi...  14.5 us
    all_to_all x2, starting transfers between devices, sent_to_all(): lax.all_to_all(jnp.broadcast_to(array[None], (length, *array.shape)), axi...  13.3 us
    reduce_scatter x1, waiting for transfers between devices, scatter_pairs(): parts = lax.psum_scatter(parts, core, scatter_dimension=0, tiled=True)  10.4 us
  transfers between devices with their start and end apart: 5, of which 5 were waited for; matrix products, arithmetic and copies ran while one was open for 9% of the time, Pallas kernels for 0%

profile of v1, /device:TPU:1, one launch (start us, length us, event | category | flops | bytes accessed | tf_op | source)
XLA Modules:
  0.0 280.5 jit_solution(12561283472467367502)
XLA Ops:
  7.2 0.0 copy-start
  7.2 1.9 broadcast_in_dim.6
  9.1 10.0 %all-to-all-start = ((bf16[16,96,256]{2,1,0:T(8,128)(2,1)}), bf16[16,96,256]{2,1,0:T(8,128)(2,1)S(1)}, u32[]{:S(2)}, u32[]{:S(2)}) async-start(bf16[16,96,256]{2,1,0:T(8,128)(2,1)} %broadcast_in_dim.6), calls=%async_computation | async-start | bytes 1572864 | tf_op jit(solution)/shard_map/all_to_all | solution.py:15
  19.1 0.7 mul.175
  19.8 1.3 copy.69
  21.1 2.3 copy.66
  23.4 0.0 copy-done.12
  23.4 6.1 %copy.67 = f32[96,2,4096]{0,2,1:T(8,128)} copy(f32[96,2,4096]{2,1,0:T(2,128)} %param.17) | data formatting | bytes 6291456 | tf_op args[1]
  29.5 1.3 copy.70
  30.8 2.3 copy.71
  33.1 8.7 %all-to-all-done = bf16[16,96,256]{2,1,0:T(8,128)(2,1)S(1)} async-done(((bf16[16,96,256]{2,1,0:T(8,128)(2,1)}), bf16[16,96,256]{2,1,0:T(8,128)(2,1)S(1)}, u32[]{:S(2)}, u32[]{:S(2)}) %all-to-all-start) | async-done | bytes 786464 | tf_op jit(solution)/shard_map/all_to_all | solution.py:15
  41.8 0.3 fusion
  42.0 0.3 fusion.7
  42.3 0.4 copy.65
  42.8 0.4 reshape.141
  43.1 1.7 multiply_reduce_fusion.4
  44.8 1.7 multiply_reduce_fusion.5
  46.5 0.0 copy-start.8
  46.5 0.0 copy-start.9
  46.5 0.2 convert_bitcast_fusion
  46.7 0.2 copy.90
  46.9 0.4 copy-done.8
  47.2 1.5 fusion.6
  48.7 0.0 copy-start.2
  48.7 1.3 fusion.12
  50.1 0.6 multiply_reduce_fusion.1
  50.7 0.5 fusion.3
  51.2 0.0 copy-start.3
  51.2 0.0 copy-start.10
  51.2 3.0 %broadcast_multiply_fusion = (f32[96,2,64,64]{0,3,2,1:T(8,128)}, f32[96,2,64]{0,2,1:T(8,128)S(1)}) fusion(f32[96,2,64]{0,2,1:T(8,128)S(1)} %fusion.3, f32[96,2,64]{0,2,1:T(8,128)S(1)} %get-tuple-element.19, f32[96,2,64,64]{0,3,2,1:T(8,128)S(1)} %bitcast.54, f32[96,2]{0,1:T(2,128)S(1)} %fusion.12, f32[96,2,64]{0,2,1:T(8,128)S(1)} %get-tuple-element.18), kind=kLoop, calls=%fused_computation.9 | loop fusion | flops 3919872 | bytes 6488832 | tf_op jit(solution)/shard_map/mul | solution.py:109
  54.3 0.4 multiply_convert_fusion.3
  54.8 0.0 copy-start.6
  54.8 0.4 convolution_convert_fusion
  55.2 0.0 copy-start.7
  55.2 0.1 copy.92
  55.3 25.8 %all_to_all.31 = bf16[16,96,256]{2,1,0:T(8,128)(2,1)S(1)} all-to-all(bf16[16,96,256]{2,1,0:T(8,128)(2,1)S(1)} %bitcast.66), channel_id=1, replica_groups=mesh['kv'=16,'tp_0'=8,'tp_1'=2] {'tp_0','tp_1'}, dimensions={0} | all-to-all | bytes 1572864 | tf_op jit(solution)/shard_map/all_to_all | solution.py:38
  81.1 0.1 convert_reduce_fusion.1
  81.2 0.1 multiply_reduce_fusion.2
  81.3 0.6 broadcast_in_dim.7
  82.0 3.4 %all-to-all-start.2 = ((f32[16,1,96]{2,1,0:T(1,128)}), f32[16,1,96]{2,1,0:T(1,128)S(1)}, u32[]{:S(2)}, u32[]{:S(2)}) async-start(f32[16,1,96]{2,1,0:T(1,128)} %broadcast_in_dim.7), calls=%async_computation.2 | async-start | bytes 16384 | tf_op jit(solution)/shard_map/all_to_all | solution.py:15
  85.3 0.0 reduce-scatter.3.cloned.1.call-start
  85.4 0.8 dynamic_slice.11
  86.2 5.8 %all-to-all-done.2 = f32[16,1,96]{2,1,0:T(1,128)S(1)} async-done(((f32[16,1,96]{2,1,0:T(1,128)}), f32[16,1,96]{2,1,0:T(1,128)S(1)}, u32[]{:S(2)}, u32[]{:S(2)}) %all-to-all-start.2) | async-done | bytes 6176 | tf_op jit(solution)/shard_map/all_to_all | solution.py:15
  91.9 0.1 multiply_convert_fusion.2
  92.0 0.1 broadcast_in_dim.8
  92.1 20.1 %all_to_all.32 = bf16[16,96,256]{2,1,0:T(8,128)(2,1)S(1)} all-to-all(bf16[16,96,256]{2,1,0:T(8,128)(2,1)S(1)} %broadcast_in_dim.8), channel_id=1, replica_groups=mesh['kv'=16,'tp_0'=8,'tp_1'=2] {'kv'}, dimensions={0} | all-to-all | bytes 1572864 | tf_op jit(solution)/shard_map/all_to_all | solution.py:15
  112.2 1.0 convolution_convert_fusion.1
  113.2 2.1 copy.74
  115.3 0.0 reduce-scatter.3.cloned.1.call-update
  115.3 0.0 reduce-scatter.5.cloned.1.call-start
  115.4 10.4 %reduce-scatter.3.cloned.1.call-done = bf16[8,96,1024]{2,1,0:T(8,128)(2,1)} async-done(((bf16[16,96,1024]{2,1,0:T(8,128)(2,1)}), bf16[8,96,1024]{2,1,0:T(8,128)(2,1)}) %reduce-scatter.3.cloned.1.call-update) | async-done | bytes 1572880 | tf_op jit(solution)/shard_map/reduce_scatter | solution.py:52
  125.7 0.0 reduce-scatter.5.cloned.1.call-update
  125.8 40.5 %reduce-scatter.5.cloned.1.call-done = bf16[1,96,1024]{2,1,0:T(8,128)(2,1)} async-done(((bf16[8,96,1024]{2,1,0:T(8,128)(2,1)}), bf16[1,96,1024]{2,1,0:T(8,128)(2,1)}) %reduce-scatter.5.cloned.1.call-update) | async-done | bytes 196624 | tf_op jit(solution)/shard_map/reduce_scatter | solution.py:53
  166.2 1.0 fusion.8
  167.2 0.4 stack.5
  167.6 0.0 copy-start.11
  167.6 82.3 %all_to_all.33 = bf16[16,96,1024]{2,1,0:T(8,128)(2,1)S(1)} all-to-all(bf16[16,96,1024]{2,1,0:T(8,128)(2,1)S(1)} %stack.5), channel_id=1, replica_groups=mesh['kv'=16,'tp_0'=8,'tp_1'=2] {'tp_0','tp_1'}, dimensions={0} | all-to-all | bytes 6291456 | tf_op jit(solution)/shard_map/all_to_all | solution.py:129
  249.9 2.0 convolution_convert_fusion.2
  251.8 6.5 %all-to-all-start.5 = ((bf16[16,96,256]{2,1,0:T(8,128)(2,1)}), bf16[16,96,256]{2,1,0:T(8,128)(2,1)S(1)}, u32[]{:S(2)}, u32[]{:S(2)}) async-start(bf16[16,96,256]{2,1,0:T(8,128)(2,1)} %bitcast.20), calls=%async_computation.7 | async-start | bytes 1572864 | tf_op jit(solution)/shard_map/all_to_all | solution.py:38
  258.3 5.8 %bitcast_add_fusion = f32[96,2,4096]{0,2,1:T(8,128)} fusion(f32[96,2,64,64]{0,3,2,1:T(8,128)} %get-tuple-element.12, f32[96,2,4096]{0,2,1:T(8,128)} %copy.67, f32[96,2]{0,1:T(2,128)S(1)} %fusion.12), kind=kLoop, calls=%fused_computation.1 | loop fusion | flops 1572864 | bytes 9437952 | tf_op jit(solution)/shard_map/add | solution.py:109
  264.1 6.0 %copy.76 = f32[96,2,4096]{2,1,0:T(2,128)} copy(f32[96,2,4096]{0,2,1:T(8,128)} %bitcast_add_fusion) | data formatting | bytes 6291456
  270.1 2.8 %all-to-all-done.5 = bf16[16,96,256]{2,1,0:T(8,128)(2,1)S(1)} async-done(((bf16[16,96,256]{2,1,0:T(8,128)(2,1)}), bf16[16,96,256]{2,1,0:T(8,128)(2,1)S(1)}, u32[]{:S(2)}, u32[]{:S(2)}) %all-to-all-start.5) | async-done | bytes 786464 | tf_op jit(solution)/shard_map/all_to_all | solution.py:38
  272.9 0.1 convert_reduce_fusion
  273.0 0.6 add_convert_fusion
  (24 shorter events, 0.1 us)
Async XLA Ops:
  7.2 47.6 %copy-start = (bf16[128,4096]{1,0:T(8,128)(2,1)S(1)}, bf16[128,4096]{1,0:T(8,128)(2,1)}, u32[]{:S(2)}) copy-start(bf16[128,4096]{1,0:T(8,128)(2,1)} %param.28) | copy-start | bytes 3145732
  7.2 12.6 %copy-start.4 = (bf16[4096,128]{1,0:T(8,128)(2,1)S(1)}, bf16[4096,128]{1,0:T(8,128)(2,1)}, u32[]{:S(2)}) copy-start(bf16[4096,128]{1,0:T(8,128)(2,1)} %param.19) | copy-start | bytes 3145732
  7.2 16.2 %copy-start.12 = (f32[2]{0:T(128)S(1)}, f32[2]{0:T(128)}, u32[]{:S(2)}) copy-start(f32[2]{0:T(128)} %param.24) | copy-start | bytes 28
  9.1 32.7 %all-to-all-start = ((bf16[16,96,256]{2,1,0:T(8,128)(2,1)}), bf16[16,96,256]{2,1,0:T(8,128)(2,1)S(1)}, u32[]{:S(2)}, u32[]{:S(2)}) async-start(bf16[16,96,256]{2,1,0:T(8,128)(2,1)} %broadcast_in_dim.6), calls=%async_computation | async-start | bytes 1572864 | tf_op jit(solution)/shard_map/all_to_all | solution.py:15
  23.4 6.1 %copy-start.5 = (bf16[4096,128]{1,0:T(8,128)(2,1)S(1)}, bf16[4096,128]{1,0:T(8,128)(2,1)}, u32[]{:S(2)}) copy-start(bf16[4096,128]{1,0:T(8,128)(2,1)} %param.20) | copy-start | bytes 3145732
  46.5 0.7 copy-start.8
  46.5 2.2 copy-start.9
  46.7 3.4 %copy-start.1 = (f32[96,2,4096]{0,2,1:T(8,128)S(1)}, f32[96,2,4096]{0,2,1:T(8,128)}, u32[]{:S(2)}) copy-start(f32[96,2,4096]{0,2,1:T(8,128)} %copy.67) | copy-start | bytes 9437188
  48.7 2.0 copy-start.2
  51.2 3.1 %copy-start.3 = (bf16[4096,128]{0,1:T(8,128)(2,1)S(1)}, bf16[4096,128]{0,1:T(8,128)(2,1)}, u32[]{:S(2)}) copy-start(bf16[4096,128]{0,1:T(8,128)(2,1)} %copy.71) | copy-start | bytes 3145732
  51.2 3.1 %copy-start.10 = (f32[64]{0:T(128)S(1)}, f32[64]{0:T(128)}, u32[]{:S(2)}) copy-start(f32[64]{0:T(128)} %param.27) | copy-start | bytes 772
  54.8 26.5 %copy-start.6 = (bf16[96,256]{1,0:T(8,128)(2,1)S(1)}, bf16[96,256]{1,0:T(8,128)(2,1)}, u32[]{:S(2)}) copy-start(bf16[96,256]{1,0:T(8,128)(2,1)} %param.16) | copy-start | bytes 147460
  55.2 57.0 %copy-start.7 = (bf16[256,1024]{1,0:T(8,128)(2,1)S(1)}, bf16[256,1024]{1,0:T(8,128)(2,1)}, u32[]{:S(2)}) copy-start(bf16[256,1024]{1,0:T(8,128)(2,1)} %param.30) | copy-start | bytes 1572868
  82.0 10.0 %all-to-all-start.2 = ((f32[16,1,96]{2,1,0:T(1,128)}), f32[16,1,96]{2,1,0:T(1,128)S(1)}, u32[]{:S(2)}, u32[]{:S(2)}) async-start(f32[16,1,96]{2,1,0:T(1,128)} %broadcast_in_dim.7), calls=%async_computation.2 | async-start | bytes 16384 | tf_op jit(solution)/shard_map/all_to_all | solution.py:15
  85.3 40.4 %reduce-scatter.3.cloned.1.call-start = ((), (), s32[]{:S(2)}) async-start(), calls=%async_computation.8 | async-start | bytes 4718592 | tf_op jit(solution)/shard_map/reduce_scatter | solution.py:52
  115.3 50.9 %reduce-scatter.5.cloned.1.call-start = ((), (), s32[]{:S(2)}) async-start(), calls=%async_computation.9 | async-start | bytes 1769472 | tf_op jit(solution)/shard_map/reduce_scatter | solution.py:53
  167.6 82.3 %copy-start.11 = (bf16[1024,256]{1,0:T(8,128)(2,1)S(1)}, bf16[1024,256]{1,0:T(8,128)(2,1)}, u32[]{:S(2)}) copy-start(bf16[1024,256]{1,0:T(8,128)(2,1)} %param.31) | copy-start | bytes 1572868
  251.8 21.1 %all-to-all-start.5 = ((bf16[16,96,256]{2,1,0:T(8,128)(2,1)}), bf16[16,96,256]{2,1,0:T(8,128)(2,1)S(1)}, u32[]{:S(2)}, u32[]{:S(2)}) async-start(bf16[16,96,256]{2,1,0:T(8,128)(2,1)} %bitcast.20), calls=%async_computation.7 | async-start | bytes 1572864 | tf_op jit(solution)/shard_map/all_to_all | solution.py:38
Sparse Core Ops, SparseCore 0:
  115.5 10.2 reduce-scatter.2
  128.3 37.8 reduce-scatter.4
